TPU v7x, 32 devices: a whole 2x2x4 slice. The times are simulated.
32 devices in a mesh: sp: 8 (over z, y), tp: 4 (over x, core).
Axes of the slice: x: 2, y: 2, z: 4, core: 2. Of those that a mesh axis runs over, the one named last changes fastest.
Arguments:
- tokens: bfloat16 [8192, 2048], P('sp'), may hold values from -6 to 6
- norm_gain: float32 [2048], replicated, may hold values from 0.1 to 1.9
- w_query: bfloat16 [2048, 1024], P('sp', 'tp'), may hold values from -3.5 to 3.5
- w_key: bfloat16 [2048, 256], P('sp', 'tp'), may hold values from -0.125 to 0.125
- w_value: bfloat16 [2048, 256], P('sp', 'tp'), may hold values from -0.125 to 0.125
- w_content: bfloat16 [2048, 1024], P('sp', 'tp'), may hold values from -0.125 to 0.125
- w_gate: bfloat16 [2048, 1024], P('sp', 'tp'), may hold values from -0.125 to 0.125
- sink_logit: float32 [16], P('tp'), may hold values from 1 to 6
- conv_weight: float32 [31, 1024], P(None, 'tp'), may hold values from -10 to 10
- conv_bias: float32 [1024], P('tp'), may hold values from 0 to 20
- channel_gain: float32 [1024], P('tp'), may hold values from 0.1 to 1.9
- out_attn: bfloat16 [1024, 2048], P('tp', 'sp'), may hold values from -0.75 to 0.75
- out_conv: bfloat16 [1024, 2048], P('tp', 'sp'), may hold values from -0.1875 to 0.1875
Outputs:
- mixed: bfloat16 [8192, 2048], P(('sp', 'tp'))
All inputs are finite; a program needn't handle non-finite values.
Results may differ from a plain program's by a relative error of at most 0.025.
The roundings to bfloat16 on the way count: a program that leaves them out, or rounds other values in their place, can miss the bound.
Values may be sent and summed in bfloat16 or wider, within the bound.
A program may use at most 64 MiB of HBM per device.

v0:
```python
import math
import jax
import jax.numpy as jnp
from jax import lax
from jax.sharding import PartitionSpec as P

HEAD_DIM = 64
CONV_CH = 1024
KERNEL = 31
WINDOW = 128
EPS = 1e-05
THETA = 10000.0


def shifted(block, axis, distance):
    devices = range(lax.axis_size(axis))
    route = [(i - distance, i) for i in devices if i - distance in devices]
    return lax.ppermute(block, axis, route)


def rotate(heads_in, positions):
    half_dim = heads_in.shape[-1] // 2
    inverse = 1.0 / THETA ** (jnp.arange(half_dim, dtype=jnp.float32) * 2.0 / heads_in.shape[-1])
    angles = positions.astype(jnp.float32)[:, None] * inverse[None, :]
    cosine = jnp.cos(angles)[:, None, :]
    sine_part = jnp.sin(angles)[:, None, :]
    former = heads_in[..., :half_dim]
    latter = heads_in[..., half_dim:]
    return jnp.concatenate(
        [former * cosine - latter * sine_part, latter * cosine + former * sine_part], axis=-1
    )


def shards(
    tokens,
    norm_gain,
    w_query,
    w_key,
    w_value,
    w_content,
    w_gate,
    sink_logit,
    conv_weight,
    conv_bias,
    channel_gain,
    out_attn,
    out_conv,
):
    token_count = tokens.shape[0]
    offset = lax.axis_index("sp") * token_count
    positions = offset + jnp.arange(token_count, dtype=jnp.int32)
    tokens_wide = tokens.astype(jnp.float32)
    inv_rms = lax.rsqrt(jnp.mean(tokens_wide * tokens_wide, axis=1, keepdims=True) + EPS)
    scaled = (tokens_wide * norm_gain[None, :]).astype(jnp.bfloat16)
    widths = [
        w_query.shape[1],
        w_key.shape[1],
        w_value.shape[1],
        w_content.shape[1],
        w_gate.shape[1],
    ]
    whole_weights = (
        lax.all_gather(w_query, "sp", axis=0, tiled=True),
        lax.all_gather(w_key, "sp", axis=0, tiled=True),
        lax.all_gather(w_value, "sp", axis=0, tiled=True),
        lax.all_gather(w_content, "sp", axis=0, tiled=True),
        lax.all_gather(w_gate, "sp", axis=0, tiled=True),
    )
    joined_whole = jnp.concatenate(whole_weights, axis=1)
    projected = jnp.dot(scaled, joined_whole, preferred_element_type=jnp.float32)
    projected = projected * inv_rms
    bounds = [0]
    for width in widths:
        bounds.append(bounds[-1] + width)
    proj_query = projected[:, bounds[0] : bounds[1]]
    proj_key = projected[:, bounds[1] : bounds[2]]
    proj_value = projected[:, bounds[2] : bounds[3]]
    proj_content = projected[:, bounds[3] : bounds[4]]
    proj_gate = projected[:, bounds[4] : bounds[5]]
    kv_local = widths[1] // HEAD_DIM
    heads_local = widths[0] // HEAD_DIM
    group_size = heads_local // kv_local
    queries = rotate(proj_query.reshape(token_count, heads_local, HEAD_DIM), positions).astype(
        jnp.bfloat16
    )
    key_rows = rotate(proj_key.reshape(token_count, kv_local, HEAD_DIM), positions).astype(
        jnp.bfloat16
    )
    value_rows = proj_value.astype(jnp.bfloat16).reshape(token_count, kv_local, HEAD_DIM)
    glu_out = (proj_content * jax.nn.sigmoid(proj_gate)).astype(jnp.bfloat16)
    prior_key, prior_value, prior_glu = shifted(
        (
            key_rows[token_count - WINDOW :],
            value_rows[token_count - WINDOW :],
            glu_out[token_count - (KERNEL - 1) :],
        ),
        "sp",
        1,
    )
    key_ext = jnp.concatenate([prior_key, key_rows], 0)
    value_ext = jnp.concatenate([prior_value, value_rows], 0)
    block_rows = math.gcd(token_count, 512)
    sink_col = sink_logit.reshape(kv_local, group_size)[:, :, None, None]

    def attend(block_start):
        query_blk = lax.dynamic_slice_in_dim(queries, block_start, block_rows, 0).reshape(
            block_rows, kv_local, group_size, HEAD_DIM
        )
        key_blk = lax.dynamic_slice_in_dim(key_ext, block_start, block_rows + WINDOW, 0)
        value_blk = lax.dynamic_slice_in_dim(value_ext, block_start, block_rows + WINDOW, 0)
        scores = jnp.einsum(
            "qkgd,jkd->kgqj", query_blk, key_blk, preferred_element_type=jnp.float32
        ) * HEAD_DIM ** (-0.5)
        query_pos = offset + block_start + jnp.arange(block_rows, dtype=jnp.int32)
        key_pos = offset + block_start - WINDOW + jnp.arange(block_rows + WINDOW, dtype=jnp.int32)
        distance = query_pos[:, None] - key_pos[None, :]
        allowed = (distance >= 0) & (distance < WINDOW) & (key_pos[None, :] >= 0)
        scores = jnp.where(allowed[None, None], scores, -1e30)
        row_max = jnp.maximum(jnp.max(scores, axis=-1, keepdims=True), sink_col)
        weights = jnp.exp(scores - row_max)
        denominator = jnp.sum(weights, axis=-1, keepdims=True) + jnp.exp(sink_col - row_max)
        probability = (weights / denominator).astype(jnp.bfloat16)
        attended = jnp.einsum(
            "kgqj,jkd->qkgd", probability, value_blk, preferred_element_type=jnp.float32
        )
        return attended.reshape(block_rows, heads_local * HEAD_DIM).astype(jnp.bfloat16)

    starts = jnp.arange(0, token_count, block_rows, dtype=jnp.int32)
    attn_out = lax.map(attend, starts).reshape(token_count, heads_local * HEAD_DIM)
    padded = jnp.concatenate([prior_glu, glu_out], 0)
    conv_sum = jnp.zeros(glu_out.shape, jnp.float32) + conv_bias[None, :]
    for tap_index in range(KERNEL):
        window_rows = lax.slice_in_dim(padded, tap_index, tap_index + token_count, axis=0)
        conv_sum = conv_sum + conv_weight[tap_index][None, :] * window_rows.astype(jnp.float32)
    row_sum, row_squares = lax.psum(
        (jnp.sum(conv_sum, axis=1), jnp.sum(conv_sum * conv_sum, axis=1)), "tp"
    )
    centre = row_sum / CONV_CH
    variance = jnp.maximum(row_squares / CONV_CH - centre * centre, 0.0)
    centred = conv_sum - centre[:, None]
    conv_out = jax.nn.silu(
        centred * lax.rsqrt(variance + EPS)[:, None] * channel_gain[None, :]
    ).astype(jnp.bfloat16)
    attn_weight, conv_weight_out = (
        lax.all_gather(out_attn, "sp", axis=1, tiled=True),
        lax.all_gather(out_conv, "sp", axis=1, tiled=True),
    )
    return lax.psum_scatter(
        (
            jnp.dot(attn_out, attn_weight, preferred_element_type=jnp.float32)
            + jnp.dot(conv_out, conv_weight_out, preferred_element_type=jnp.float32)
        ).astype(jnp.bfloat16),
        "tp",
        scatter_dimension=0,
        tiled=True,
    )


def solution(mesh):
    placed = (
        P("sp", None),
        P(),
        P("sp", "tp"),
        P("sp", "tp"),
        P("sp", "tp"),
        P("sp", "tp"),
        P("sp", "tp"),
        P("tp"),
        P(None, "tp"),
        P("tp"),
        P("tp"),
        P("tp", "sp"),
        P("tp", "sp"),
    )
    return jax.shard_map(
        shards, mesh=mesh, in_specs=placed, out_specs=P(("sp", "tp"), None), check_vma=False
    )
```

profile of v0, /device:TPU:0, one launch (start us, length us, event | category | flops | bytes accessed | tf_op | source)
XLA Modules:
  0.0 276.7 jit_solution(9602372100434839561)
XLA Ops:
  12.0 3.1 %fusion.20 = f32[1024]{0:T(1024)S(1)} fusion(bf16[1024,2048]{1,0:T(8,128)(2,1)} %param.15), kind=kLoop, calls=%fused_computation.31 | loop fusion | flops 6290432 | bytes 4198400 | tf_op jit(solution)/shard_map/reduce_sum | solution.py:53
  16.9 33.8 %all_gather.23 = bf16[2048,64]{1,0:T(8,128)(2,1)S(1)} all-gather(bf16[256,64]{1,0:T(8,128)(2,1)S(1)} %copy.19), channel_id=1, replica_groups=mesh['sp'=8,'tp'=4] {'sp'}, dimensions={0}, use_global_device_ids=true | all-gather | bytes 294912 | tf_op jit(solution)/shard_map/all_gather | solution.py:65
  50.6 31.7 %all_gather.22 = bf16[2048,64]{1,0:T(8,128)(2,1)S(1)} all-gather(bf16[256,64]{1,0:T(8,128)(2,1)S(1)} %copy.18), channel_id=1, replica_groups=mesh['sp'=8,'tp'=4] {'sp'}, dimensions={0}, use_global_device_ids=true | all-gather | bytes 294912 | tf_op jit(solution)/shard_map/all_gather | solution.py:64
  83.0 14.4 %all-gather.8.cloned.1.call-done = bf16[2048,256]{1,0:T(8,128)(2,1)} async-done(((bf16[256,256]{1,0:T(8,128)(2,1)}), bf16[2048,256]{1,0:T(8,128)(2,1)}) %all-gather.8.cloned.1.call-update) | async-done | bytes 1048592 | tf_op jit(solution)/shard_map/all_gather | solution.py:66
  97.4 41.2 %all-gather.10.cloned.1.call-done = bf16[2048,256]{1,0:T(8,128)(2,1)} async-done(((bf16[256,256]{1,0:T(8,128)(2,1)}), bf16[2048,256]{1,0:T(8,128)(2,1)}) %all-gather.10.cloned.1.call-update) | async-done | bytes 1048592 | tf_op jit(solution)/shard_map/all_gather | solution.py:67
  138.5 6.7 %concatenate.28 = bf16[2048,896]{1,0:T(8,128)(2,1)} concatenate(bf16[2048,256]{1,0:T(8,128)(2,1)} %all-gather.6.cloned.1.call-done, bf16[2048,64]{1,0:T(8,128)(2,1)S(1)} %all_gather.22, bf16[2048,64]{1,0:T(8,128)(2,1)S(1)} %all_gather.23, bf16[2048,256]{1,0:T(8,128)(2,1)} %all-gather.8.cloned.1.call-done, bf16[2048,256]{1,0:T(8,128)(2,1)} %all-gather.10.cloned.1.call-done), dimensions={1} | concatenate | bytes 7340032 | tf_op jit(solution)/shard_map/concatenate | solution.py:69
  145.2 7.0 %fusion.77 = (bf16[1024,896]{0,1:T(8,128)(2,1)S(1)}, f32[1024,896]{0,1:T(8,128)S(1)}) fusion(f32[1024]{0:T(1024)S(1)} %add_rsqrt_fusion.1, bf16[2048,896]{1,0:T(8,128)(2,1)} %concatenate.28, bf16[1024,2048]{1,0:T(8,128)(2,1)} %param.15, f32[2048]{0:T(1024)S(1)} %copy-done.3), kind=kOutput, calls=%fused_computation.147 | convolution fusion | flops 3766222848 | bytes 13381632 | tf_op jit(solution)/shard_map/dot_general | solution.py:70
  152.6 2.4 collective-permute-start
  155.6 3.1 %collective-permute-start.1 = (bf16[128,1,64]{0,2,1:T(8,128)(2,1)S(1)}, bf16[128,1,64]{0,2,1:T(8,128)(2,1)S(1)}, u32[]{:S(2)}, u32[]{:S(2)}) collective-permute-start(bf16[128,1,64]{0,2,1:T(8,128)(2,1)S(1)} %pad_maximum_fusion.3), channel_id=1, source_target_pairs={{0,4},{4,8},{8,12},{12,16},{16,20},{20,24},{24,28},{1,5},{5,9},{9,... | collective-permute-start | bytes 49160 | tf_op jit(solution)/shard_map/ppermute | solution.py:18
  158.8 2.5 collective-permute-start.2
  161.6 1.7 collective-permute-done.2
  163.3 7.8 %fusion.74 = (f32[1024]{0:T(1024)S(1)}, f32[1024]{0:T(1024)S(1)}, f32[1024,256]{0,1:T(8,128)S(1)}) fusion(bf16[1024,256]{0,1:T(8,128)(2,1)S(1)} %get-tuple-element.130, f32[256]{0:T(256)S(1)} %bitcast.115, bf16[30,256]{0,1:T(8,128)(2,1)S(1)} %collective-permute-done.2, f32[256]{0:T(256)S(1)} %bitcast.116, f32[256]{0:T(256)S(1)} %bitcast.118, ...), kind=kLoop, calls=%fused_computation.144 | loop fusion | flops 48756736 | bytes 1629184 | tf_op jit(solution)/shard_map/reduce_sum | solution.py:136
  171.1 6.1 %all-reduce = (f32[1024]{0:T(1024)S(1)}, f32[1024]{0:T(1024)S(1)}) all-reduce(f32[1024]{0:T(1024)S(1)} %get-tuple-element.108, f32[1024]{0:T(1024)S(1)} %get-tuple-element.107), channel_id=1, replica_groups=mesh['sp'=8,'tp'=4] {'tp'}, use_global_device_ids=true, to_apply=%region_8.9 | all-reduce | flops 2048 | bytes 16384 | tf_op jit(solution)/shard_map/psum | solution.py:135
  177.3 18.4 %while.12 = (s32[]{:T(128)}, bf16[2,512,256]{2,1,0:T(8,128)(2,1)S(1)}, s32[2]{0:T(128)S(1)}, bf16[1152,1,64]{0,2,1:T(8,128)(2,1)S(1)}, s32[]{:T(128)}, /*index=5...) while((s32[]{:T(128)}, ...), condition=%wide.region_4.5_spmd, body=%wide.region_1.4_spmd.sunk | while | flops 353048960 | bytes 18868768 | solution.py:129
  182.1 1.2 fusion.92
  183.4 1.1 fusion.93
  184.6 1.7 fusion.94
  191.3 1.2 fusion.92
  192.6 1.1 fusion.93
  193.8 1.7 fusion.94
  195.7 5.7 %fusion.78 = f32[1024,2048]{1,0:T(8,128)} fusion(bf16[1024,256]{1,0:T(8,128)(2,1)S(1)} %bitcast.101, bf16[256,2048]{1,0:T(8,128)(2,1)} %all-gather.12.cloned.1.call-done), kind=kOutput, calls=%fused_computation.148 | convolution fusion | flops 1073741824 | bytes 9961472 | tf_op jit(solution)/shard_map/dot_general | solution.py:150
  201.5 17.5 %all-gather.14.cloned.1.call-done = bf16[256,2048]{1,0:T(8,128)(2,1)} async-done(((bf16[256,256]{1,0:T(8,128)(2,1)}), bf16[256,2048]{1,0:T(8,128)(2,1)}) %all-gather.14.cloned.1.call-update) | async-done | bytes 1048592 | tf_op jit(solution)/shard_map/all_gather | solution.py:146
  218.9 7.2 %add_convert_fusion = bf16[1024,2048]{1,0:T(8,128)(2,1)} fusion(f32[1024,2048]{1,0:T(8,128)} %fusion.78, bf16[256,2048]{1,0:T(8,128)(2,1)} %all-gather.14.cloned.1.call-done, f32[1024,256]{0,1:T(8,128)S(1)} %get-tuple-element.127, f32[256]{0:T(256)S(1)} %copy-done.2, f32[1024]{0:T(1024)S(1)} %get-tuple-element.170, f32[1024]{0:T(1024)S(1)} %get-tuple-element.169), kind=kOutput, calls=%fused_computation.32 | convolution fusion | flops 1080033280 | bytes 14689280 | tf_op jit(solution)/shard_map/dot_general | solution.py:151
  226.1 43.7 %reduce-scatter.2.cloned.1.call-done = bf16[256,2048]{1,0:T(8,128)(2,1)} async-done(((bf16[1024,2048]{1,0:T(8,128)(2,1)}), bf16[256,2048]{1,0:T(8,128)(2,1)}) %reduce-scatter.2.cloned.1.call-update) | async-done | bytes 1048592 | tf_op jit(solution)/shard_map/reduce_scatter | solution.py:148
  (64 shorter events, 11.7 us)
Async XLA Ops:
  6.5 76.4 %all-gather.6.cloned.1.call-start = ((), (), s32[]{:S(2)}) async-start(), calls=%async_computation.1 | async-start | bytes 1179648 | tf_op jit(solution)/shard_map/all_gather | solution.py:63
  7.3 90.1 %all-gather.8.cloned.1.call-start = ((), (), s32[]{:S(2)}) async-start(), calls=%async_computation.2 | async-start | bytes 1179648 | tf_op jit(solution)/shard_map/all_gather | solution.py:66
  8.0 130.5 %all-gather.10.cloned.1.call-start = ((), (), s32[]{:S(2)}) async-start(), calls=%async_computation.3 | async-start | bytes 1179648 | tf_op jit(solution)/shard_map/all_gather | solution.py:67
  8.7 187.0 %all-gather.12.cloned.1.call-start = ((), (), s32[]{:S(2)}) async-start(), calls=%async_computation.4 | async-start | bytes 1179648 | tf_op jit(solution)/shard_map/all_gather | solution.py:145
  9.3 209.6 %all-gather.14.cloned.1.call-start = ((), (), s32[]{:S(2)}) async-start(), calls=%async_computation.5 | async-start | bytes 1179648 | tf_op jit(solution)/shard_map/all_gather | solution.py:146
  9.9 260.0 %reduce-scatter.2.cloned.1.call-start = ((), (), s32[]{:S(2)}) async-start(), calls=%async_computation.6 | async-start | bytes 5242880 | tf_op jit(solution)/shard_map/reduce_scatter | solution.py:148
  15.1 130.1 %copy-start.3 = (f32[2048]{0:T(1024)S(1)}, f32[2048]{0:T(1024)}, u32[]{:S(2)}) copy-start(f32[2048]{0:T(1024)} %param.16) | copy-start | bytes 24580
  152.2 11.0 %copy-start.1 = (f32[256]{0:T(256)S(1)}, f32[256]{0:T(256)}, u32[]{:S(2)}) copy-start(f32[256]{0:T(256)} %param.24) | copy-start | bytes 3076
  152.3 25.0 %copy-start = (f32[4]{0:T(128)S(1)}, f32[4]{0:T(128)}, u32[]{:S(2)}) copy-start(f32[4]{0:T(128)} %param.22) | copy-start | bytes 52
  152.6 24.6 %collective-permute-start = (bf16[128,1,64]{0,2,1:T(8,128)(2,1)S(1)}, bf16[128,1,64]{0,2,1:T(8,128)(2,1)S(1)}, u32[]{:S(2)}, u32[]{:S(2)}) collective-permute-start(bf16[128,1,64]{0,2,1:T(8,128)(2,1)S(1)} %slice_bitcast_fusion.2), channel_id=1, source_target_pairs={{0,4},{4,8},{8,12},{12,16},{16,20},{20,24},{24,28},{1,5},{5,9},{9,... | collective-permute-start | bytes 49160 | tf_op jit(solution)/shard_map/ppermute | solution.py:18
  155.6 21.6 %collective-permute-start.1 = (bf16[128,1,64]{0,2,1:T(8,128)(2,1)S(1)}, bf16[128,1,64]{0,2,1:T(8,128)(2,1)S(1)}, u32[]{:S(2)}, u32[]{:S(2)}) collective-permute-start(bf16[128,1,64]{0,2,1:T(8,128)(2,1)S(1)} %pad_maximum_fusion.3), channel_id=1, source_target_pairs={{0,4},{4,8},{8,12},{12,16},{16,20},{20,24},{24,28},{1,5},{5,9},{9,... | collective-permute-start | bytes 49160 | tf_op jit(solution)/shard_map/ppermute | solution.py:18
  158.8 4.4 %collective-permute-start.2 = (bf16[30,256]{0,1:T(8,128)(2,1)S(1)}, bf16[30,256]{0,1:T(8,128)(2,1)S(1)}, u32[]{:S(2)}, u32[]{:S(2)}) collective-permute-start(bf16[30,256]{0,1:T(8,128)(2,1)S(1)} %slice.308), channel_id=1, source_target_pairs={{0,4},{4,8},{8,12},{12,16},{16,20},{20,24},{24,28},{1,5},{5,9},{9,... | collective-permute-start | bytes 46088 | tf_op jit(solution)/shard_map/ppermute | solution.py:18
  195.7 23.2 %copy-start.2 = (f32[256]{0:T(256)S(1)}, f32[256]{0:T(256)}, u32[]{:S(2)}) copy-start(f32[256]{0:T(256)} %param.25) | copy-start | bytes 3076
Sparse Core Ops, SparseCore 0:
  9.5 45.0 all-gather.5
  56.6 40.6 all-gather.7
  99.5 38.9 all-gather.9
  140.4 38.1 all-gather.11
  180.5 38.3 all-gather.13
  226.3 43.5 reduce-scatter.1
where the time goes:
time: 278 us; the launch traced here: 277 us
  waiting for transfers between devices  122 us (44%)
  blocking collectives  71.6 us (26%)
  matrix products  25.7 us (9%)
  other arithmetic  15.9 us (6%)
  between operations  13.7 us (5%)
  local copies, waits for them, and re-layouts  12.2 us (4%)
  starting transfers between devices  8.25 us (3%)
  loops' own time  7.56 us (3%)
    reduce_scatter x1, waiting for transfers between devices, shards(): lax.psum_scatter((jnp.dot(attn_out, attn_weight, preferred_element_type=j...  43.7 us
    all_gather x1, waiting for transfers between devices, shards(): lax.all_gather(w_gate, 'sp', axis=0, tiled=True)  41.2 us
    all_gather x1, blocking collectives, shards(): lax.all_gather(w_value, 'sp', axis=0, tiled=True)  33.8 us
    all_gather x1, blocking collectives, shards(): lax.all_gather(w_key, 'sp', axis=0, tiled=True)  31.7 us
    all_gather x1, waiting for transfers between devices, shards(): lax.all_gather(out_conv, 'sp', axis=1, tiled=True)  17.5 us
    all_gather x1, waiting for transfers between devices, shards(): lax.all_gather(w_content, 'sp', axis=0, tiled=True)  14.4 us
    ppermute x3, starting transfers between devices, shifted(): return lax.ppermute(block, axis, route)  8.06 us
    reduce_sum x1, other arithmetic, shards(): jnp.sum(conv_sum, axis=1)  7.81 us
  transfers between devices with their start and end apart: 9, of which 5 were waited for; matrix products, arithmetic and copies ran while one was open for 17% of the time, Pallas kernels for 0%

commit v1 on v0

--- a/solution.py
+++ b/solution.py
@@ -141,9 +141,14 @@
     conv_out = jax.nn.silu(
         centred * lax.rsqrt(variance + EPS)[:, None] * channel_gain[None, :]
     ).astype(jnp.bfloat16)
+
+    def open_boxes(inp, link_axis):
+        b_now = jnp.concatenate(lax.all_gather(inp, link_axis), 1)
+        return b_now
+
     attn_weight, conv_weight_out = (
         lax.all_gather(out_attn, "sp", axis=1, tiled=True),
-        lax.all_gather(out_conv, "sp", axis=1, tiled=True),
+        open_boxes(out_conv, "sp"),
     )
     return lax.psum_scatter(
         (

time: 278 us -> 291 us (1.047)
  waiting for transfers between devices: 122 us -> 134 us
  matrix products: 25.7 us -> 19.1 us
  local copies, waits for them, and re-layouts: 12.2 us -> 16.9 us
    all_gather x1, waiting for transfers between devices: 17.5 us -> 26.9 us  [open_boxes(): b_now = jnp.concatenate(lax.all_gather(inp, link_axis), 1)]
    dot_general x1, matrix products: 7.17 us -> 3.6 us  [shards(): jnp.dot(conv_out, conv_weight_out, preferred_element_type=jnp.float32)]
    dot_general x1, matrix products: 5.72 us -> 2.65 us  [shards(): jnp.dot(attn_out, attn_weight, preferred_element_type=jnp.float32)]
    reduce_scatter x1, waiting for transfers between devices: 43.7 us -> 46.7 us  [shards(): lax.psum_scatter((jnp.dot(attn_out, attn_weight, preferred_element_type=j...]
where the time goes in v1:
time: 291 us; the launch traced here: 290 us
  waiting for transfers between devices  134 us (46%)
  blocking collectives  71.6 us (25%)
  matrix products  19.1 us (7%)
  other arithmetic  18.3 us (6%)
  local copies, waits for them, and re-layouts  16.9 us (6%)
  between operations  13.7 us (5%)
  starting transfers between devices  8.37 us (3%)
  loops' own time  7.57 us (3%)
    reduce_scatter x1, waiting for transfers between devices, shards(): lax.psum_scatter((jnp.dot(attn_out, attn_weight, preferred_element_type=j...  46.7 us
    all_gather x1, waiting for transfers between devices, shards(): lax.all_gather(w_gate, 'sp', axis=0, tiled=True)  41.2 us
    all_gather x1, blocking collectives, shards(): lax.all_gather(w_value, 'sp', axis=0, tiled=True)  34.2 us
    all_gather x1, blocking collectives, shards(): lax.all_gather(w_key, 'sp', axis=0, tiled=True)  31.4 us
    all_gather x1, waiting for transfers between devices, open_boxes(): b_now = jnp.concatenate(lax.all_gather(inp, link_axis), 1)  26.9 us
    all_gather x1, waiting for transfers between devices, shards(): lax.all_gather(w_content, 'sp', axis=0, tiled=True)  14.7 us
    reduce_sum x1, other arithmetic, shards(): jnp.sum(conv_sum, axis=1)  8.93 us
    ppermute x3, starting transfers between devices, shifted(): return lax.ppermute(block, axis, route)  8.18 us
  transfers between devices with their start and end apart: 9, of which 5 were waited for; matrix products, arithmetic and copies ran while one was open for 17% of the time, Pallas kernels for 0%

profile of v1, /device:TPU:0, one launch (start us, length us, event | category | flops | bytes accessed | tf_op | source)
XLA Modules:
  0.0 289.9 jit_solution(11101624303992550461)
XLA Ops:
  11.5 1.6 fusion.75
  13.1 3.1 %fusion.20 = f32[1024]{0:T(1024)S(1)} fusion(bf16[1024,2048]{1,0:T(8,128)(2,1)} %param.15), kind=kLoop, calls=%fused_computation.31 | loop fusion | flops 6290432 | bytes 4198400 | tf_op jit(solution)/shard_map/reduce_sum | solution.py:53
  18.0 34.2 %all_gather.26 = bf16[2048,64]{1,0:T(8,128)(2,1)S(1)} all-gather(bf16[256,64]{1,0:T(8,128)(2,1)S(1)} %copy.23), channel_id=1, replica_groups=mesh['sp'=8,'tp'=4] {'sp'}, dimensions={0}, use_global_device_ids=true | all-gather | bytes 294912 | tf_op jit(solution)/shard_map/all_gather | solution.py:65
  52.2 31.4 %all_gather.25 = bf16[2048,64]{1,0:T(8,128)(2,1)S(1)} all-gather(bf16[256,64]{1,0:T(8,128)(2,1)S(1)} %copy.22), channel_id=1, replica_groups=mesh['sp'=8,'tp'=4] {'sp'}, dimensions={0}, use_global_device_ids=true | all-gather | bytes 294912 | tf_op jit(solution)/shard_map/all_gather | solution.py:64
  84.2 14.7 %all-gather.9.cloned.1.call-done = bf16[2048,256]{1,0:T(8,128)(2,1)} async-done(((bf16[256,256]{1,0:T(8,128)(2,1)}), bf16[2048,256]{1,0:T(8,128)(2,1)}) %all-gather.9.cloned.1.call-update) | async-done | bytes 1048592 | tf_op jit(solution)/shard_map/all_gather | solution.py:66
  98.8 41.2 %all-gather.11.cloned.1.call-done = bf16[2048,256]{1,0:T(8,128)(2,1)} async-done(((bf16[256,256]{1,0:T(8,128)(2,1)}), bf16[2048,256]{1,0:T(8,128)(2,1)}) %all-gather.11.cloned.1.call-update) | async-done | bytes 1048592 | tf_op jit(solution)/shard_map/all_gather | solution.py:67
  140.0 6.7 %concatenate.28 = bf16[2048,896]{1,0:T(8,128)(2,1)} concatenate(bf16[2048,256]{1,0:T(8,128)(2,1)} %all-gather.7.cloned.1.call-done, bf16[2048,64]{1,0:T(8,128)(2,1)S(1)} %all_gather.25, bf16[2048,64]{1,0:T(8,128)(2,1)S(1)} %all_gather.26, bf16[2048,256]{1,0:T(8,128)(2,1)} %all-gather.9.cloned.1.call-done, bf16[2048,256]{1,0:T(8,128)(2,1)} %all-gather.11.cloned.1.call-done), dimensions={1} | concatenate | bytes 7340032 | tf_op jit(solution)/shard_map/concatenate | solution.py:69
  146.7 7.0 %fusion.77 = (bf16[1024,896]{0,1:T(8,128)(2,1)S(1)}, f32[1024,896]{0,1:T(8,128)S(1)}) fusion(f32[1024]{0:T(1024)S(1)} %add_rsqrt_fusion.1, bf16[2048,896]{1,0:T(8,128)(2,1)} %concatenate.28, bf16[1024,2048]{1,0:T(8,128)(2,1)} %param.15, f32[2048]{0:T(1024)S(1)} %copy-done.2), kind=kOutput, calls=%fused_computation.147 | convolution fusion | flops 3766222848 | bytes 13381632 | tf_op jit(solution)/shard_map/dot_general | solution.py:70
  154.1 26.9 %all-gather.15.cloned.1.call-done = bf16[2048,256]{1,0:T(8,128)(2,1)} async-done(((bf16[256,256]{1,0:T(8,128)(2,1)}), bf16[2048,256]{1,0:T(8,128)(2,1)}) %all-gather.15.cloned.1.call-update) | async-done | bytes 1048592 | tf_op jit(solution)/shard_map/all_gather | solution.py:146
  181.0 1.5 copy.25
  182.5 3.1 %collective-permute-start = (bf16[128,1,64]{0,2,1:T(8,128)(2,1)S(1)}, bf16[128,1,64]{0,2,1:T(8,128)(2,1)}, u32[]{:S(2)}, u32[]{:S(2)}) collective-permute-start(bf16[128,1,64]{0,2,1:T(8,128)(2,1)S(1)} %slice_bitcast_fusion.2), channel_id=1, source_target_pairs={{0,4},{4,8},{8,12},{12,16},{16,20},{20,24},{24,28},{1,5},{5,9},{9,... | collective-permute-start | bytes 49160 | tf_op jit(solution)/shard_map/ppermute | solution.py:18
  186.1 2.5 collective-permute-start.1
  188.8 2.6 collective-permute-start.2
  191.5 1.7 collective-permute-done.2
  193.2 8.9 %fusion.74 = (f32[1024]{0:T(1024)S(1)}, f32[1024]{0:T(1024)S(1)}, f32[1024,256]{0,1:T(8,128)S(1)}) fusion(bf16[1024,256]{0,1:T(8,128)(2,1)S(1)} %get-tuple-element.130, f32[256]{0:T(256)S(1)} %bitcast.121, bf16[30,256]{0,1:T(8,128)(2,1)S(1)} %collective-permute-done.2, f32[256]{0:T(256)S(1)} %bitcast.122, f32[256]{0:T(256)S(1)} %bitcast.124, ...), kind=kLoop, calls=%fused_computation.144 | loop fusion | flops 48756736 | bytes 1629184 | tf_op jit(solution)/shard_map/reduce_sum | solution.py:136
  202.2 6.0 %all-reduce = (f32[1024]{0:T(1024)S(1)}, f32[1024]{0:T(1024)S(1)}) all-reduce(f32[1024]{0:T(1024)S(1)} %get-tuple-element.108, f32[1024]{0:T(1024)S(1)} %get-tuple-element.107), channel_id=1, replica_groups=mesh['sp'=8,'tp'=4] {'tp'}, use_global_device_ids=true, to_apply=%region_8.9 | all-reduce | flops 2048 | bytes 16384 | tf_op jit(solution)/shard_map/psum | solution.py:135
  208.9 21.1 %while.12 = (s32[]{:T(128)}, bf16[2,512,256]{2,1,0:T(8,128)(2,1)}, s32[2]{0:T(128)}, bf16[1152,1,64]{0,2,1:T(8,128)(2,1)S(1)}, s32[]{:T(128)}, /*index=5*/bf16[1...) while((s32[]{:T(128)}, bf16[2,512,256]{2,1,0:T(8,128)(2,1)}, ...), condition=%wide.region_4.5_spmd, body=%wide.region_1.4_spmd.sunk | while | flops 353048960 | bytes 18868860 | solution.py:129
  208.9 1.3 dynamic_slice.46
  216.9 1.7 fusion.94
  219.4 1.3 dynamic_slice.46
  227.4 1.7 fusion.94
  230.0 2.7 fusion.78
  232.6 3.6 %add_convert_fusion = bf16[1024,2048]{1,0:T(8,128)(2,1)} fusion(f32[1024,2048]{1,0:T(8,128)S(1)} %fusion.78, bf16[256,2048]{0,1:T(8,128)(2,1)S(1)} %bitcast.104, f32[1024,256]{0,1:T(8,128)S(1)} %get-tuple-element.127, f32[256]{0:T(256)S(1)} %copy-done.1, f32[1024]{0:T(1024)S(1)} %get-tuple-element.170, f32[1024]{0:T(1024)S(1)} %get-tuple-element.169), kind=kOutput, calls=%fused_computation.32 | convolution fusion | flops 1080033280 | bytes 14689280 | tf_op jit(solution)/shard_map/dot_general | solution.py:156
  236.3 46.7 %reduce-scatter.2.cloned.1.call-done = bf16[256,2048]{1,0:T(8,128)(2,1)} async-done(((bf16[1024,2048]{1,0:T(8,128)(2,1)}), bf16[256,2048]{1,0:T(8,128)(2,1)}) %reduce-scatter.2.cloned.1.call-update) | async-done | bytes 1048592 | tf_op jit(solution)/shard_map/reduce_scatter | solution.py:153
  (65 shorter events, 16.7 us)
Async XLA Ops:
  6.5 77.6 %all-gather.7.cloned.1.call-start = ((), (), s32[]{:S(2)}) async-start(), calls=%async_computation.1 | async-start | bytes 1179648 | tf_op jit(solution)/shard_map/all_gather | solution.py:63
  7.3 91.6 %all-gather.9.cloned.1.call-start = ((), (), s32[]{:S(2)}) async-start(), calls=%async_computation.2 | async-start | bytes 1179648 | tf_op jit(solution)/shard_map/all_gather | solution.py:66
  8.0 132.0 %all-gather.11.cloned.1.call-start = ((), (), s32[]{:S(2)}) async-start(), calls=%async_computation.3 | async-start | bytes 1179648 | tf_op jit(solution)/shard_map/all_gather | solution.py:67
  8.7 172.3 %all-gather.15.cloned.1.call-start = ((), (), s32[]{:S(2)}) async-start(), calls=%async_computation.6 | async-start | bytes 1179648 | tf_op jit(solution)/shard_map/all_gather | solution.py:146
  9.3 220.7 %all-gather.13.cloned.1.call-start = ((), (), s32[]{:S(2)}) async-start(), calls=%async_computation.4 | async-start | bytes 1179648 | tf_op jit(solution)/shard_map/all_gather | solution.py:150
  9.9 273.1 %reduce-scatter.2.cloned.1.call-start = ((), (), s32[]{:S(2)}) async-start(), calls=%async_computation.5 | async-start | bytes 5242880 | tf_op jit(solution)/shard_map/reduce_scatter | solution.py:153
  16.2 130.5 %copy-start.2 = (f32[2048]{0:T(1024)S(1)}, f32[2048]{0:T(1024)}, u32[]{:S(2)}) copy-start(f32[2048]{0:T(1024)} %param.16) | copy-start | bytes 24580
  182.5 25.7 %collective-permute-start = (bf16[128,1,64]{0,2,1:T(8,128)(2,1)S(1)}, bf16[128,1,64]{0,2,1:T(8,128)(2,1)}, u32[]{:S(2)}, u32[]{:S(2)}) collective-permute-start(bf16[128,1,64]{0,2,1:T(8,128)(2,1)S(1)} %slice_bitcast_fusion.2), channel_id=1, source_target_pairs={{0,4},{4,8},{8,12},{12,16},{16,20},{20,24},{24,28},{1,5},{5,9},{9,... | collective-permute-start | bytes 49160 | tf_op jit(solution)/shard_map/ppermute | solution.py:18
  186.1 22.0 %collective-permute-start.1 = (bf16[128,1,64]{0,2,1:T(8,128)(2,1)S(1)}, bf16[128,1,64]{0,2,1:T(8,128)(2,1)S(1)}, u32[]{:S(2)}, u32[]{:S(2)}) collective-permute-start(bf16[128,1,64]{0,2,1:T(8,128)(2,1)S(1)} %pad_maximum_fusion.3), channel_id=1, source_target_pairs={{0,4},{4,8},{8,12},{12,16},{16,20},{20,24},{24,28},{1,5},{5,9},{9,... | collective-permute-start | bytes 49160 | tf_op jit(solution)/shard_map/ppermute | solution.py:18
  188.8 4.4 %collective-permute-start.2 = (bf16[30,256]{0,1:T(8,128)(2,1)S(1)}, bf16[30,256]{0,1:T(8,128)(2,1)S(1)}, u32[]{:S(2)}, u32[]{:S(2)}) collective-permute-start(bf16[30,256]{0,1:T(8,128)(2,1)S(1)} %slice.308), channel_id=1, source_target_pairs={{0,4},{4,8},{8,12},{12,16},{16,20},{20,24},{24,28},{1,5},{5,9},{9,... | collective-permute-start | bytes 46088 | tf_op jit(solution)/shard_map/ppermute | solution.py:18
  208.9 6.7 %copy-start = (f32[1,4,1,1]{1,3,2,0:T(1,128)S(1)}, f32[1,4,1,1]{1,3,2,0:T(1,128)}, u32[]{:S(2)}) copy-start(f32[1,4,1,1]{1,3,2,0:T(1,128)} %get-tuple-element.259) | copy-start | bytes 52 | tf_op jit(solution)/shard_map/while
  219.4 6.7 %copy-start = (f32[1,4,1,1]{1,3,2,0:T(1,128)S(1)}, f32[1,4,1,1]{1,3,2,0:T(1,128)}, u32[]{:S(2)}) copy-start(f32[1,4,1,1]{1,3,2,0:T(1,128)} %get-tuple-element.259) | copy-start | bytes 52 | tf_op jit(solution)/shard_map/while
  230.0 2.7 copy-start.1
Sparse Core Ops, SparseCore 0:
  9.5 45.3 all-gather.6
  57.0 41.8 all-gather.8
  101.0 38.9 all-gather.10
  142.0 38.9 all-gather.14
  182.9 38.7 all-gather.12
  236.4 46.5 reduce-scatter.1
